TPU v7x, 32 devices: a whole 2x2x4 slice. The times are simulated.
32 devices in a mesh: sp: 8 (over z, x), tp: 4 (over y, core).
Axes of the slice: x: 2, y: 2, z: 4, core: 2. Of those that a mesh axis runs over, the one named last changes fastest.
Arguments:
- queries: bfloat16 [4096, 1024], P('sp', 'tp'), may hold values from -5.5 to 5.5
- key_vectors: bfloat16 [4096, 1024], P('sp', 'tp'), may hold values from -5.5 to 5.5
- latents: bfloat16 [4096, 2048], P('sp', 'tp'), may hold values from -6 to 6
- w_value: bfloat16 [2048, 1024], P(None, 'tp'), may hold values from -0.125 to 0.125
- log_sums: float32 [4096, 16], P('sp', 'tp'), as said below
- out_pair: bfloat16 [4096, 2048], P('sp', 'tp'), may hold values from -6 to 6
- cotangent: bfloat16 [4096, 1024], P('sp', 'tp'), may hold values from -6 to 6
- lambdas: float32 [8], P('tp'), may hold values from 0.3 to 0.8
- out_gain: float32 [128], replicated, may hold values from 0.1 to 1.9
Outputs:
- query_grad: float32 [4096, 1024], P('sp', 'tp')
- key_grad: float32 [4096, 1024], P('sp', 'tp')
- value_grad: float32 [4096, 1024], P('sp', 'tp')
- weight_grad: float32 [2048, 1024], P('sp', 'tp')
Inputs may be any that keep to these rules, and one draw needn't show every extreme that they name: `log_sums`: each entry is the logarithm of the sum of exp(scores_c[t, s]) over s <= t for its row t, head h and map c.
All inputs are finite; a program needn't handle non-finite values.
Results may differ from a plain program's by a relative error of at most 0.008.
Values may be sent and summed in bfloat16 or wider, within the bound.
A program may use at most 64 MiB of HBM per device.

v0:
```python
import jax
import jax.numpy as jnp
from jax import lax
from jax.sharding import PartitionSpec as P

norm_floor = 0.25
block_rows = 512


def head_cotangent(out_pair, cotangent, lambdas, out_gain):
    tok_rows = out_pair.shape[0]
    head_count = lambdas.shape[0]
    out_maps = out_pair.astype(jnp.float32).reshape(tok_rows, head_count, 2, -1)
    lam_cols = lambdas[None, :, None]
    merged = out_maps[:, :, 0] - lam_cols * out_maps[:, :, 1]
    inv_norm = lax.rsqrt(jnp.mean(merged * merged, axis=-1, keepdims=True) + norm_floor)
    scaled = cotangent.astype(jnp.float32).reshape(merged.shape) * out_gain
    inner_dot = jnp.mean(scaled * merged, axis=-1, keepdims=True)
    out_grad = (inv_norm * scaled - merged * (inv_norm * inv_norm * inv_norm) * inner_dot).astype(
        jnp.bfloat16
    )
    grad_wide = out_grad.astype(jnp.float32)
    first_map = jnp.sum(grad_wide * out_maps[:, :, 0], axis=-1)
    second_map = -lambdas[None, :] * jnp.sum(grad_wide * out_maps[:, :, 1], axis=-1)
    return (out_grad, jnp.stack([first_map, second_map], axis=-1))


def block_terms(
    query_block,
    key_block,
    value_block,
    grad_block,
    log_block,
    term_block,
    lambdas,
    query_pos,
    key_pos,
):
    factor = query_block.shape[-1] ** (-0.5)
    scores = (
        jnp.einsum("qhcd,khcd->hcqk", query_block, key_block, preferred_element_type=jnp.float32)
        * factor
    )
    visible = key_pos[None, :] <= query_pos[:, None]
    shifted = scores - jnp.transpose(log_block, (1, 2, 0))[..., None]
    softmax_maps = jnp.where(visible, jnp.exp(shifted), 0.0)
    value_dot = jnp.einsum(
        "qhe,khe->hqk", grad_block, value_block, preferred_element_type=jnp.float32
    )
    lam_cols = lambdas[:, None, None]
    weights = (softmax_maps[:, 0] - lam_cols * softmax_maps[:, 1]).astype(jnp.bfloat16)
    term_cols = jnp.transpose(term_block, (1, 2, 0))
    first_map = softmax_maps[:, 0] * (value_dot - term_cols[:, 0, :, None])
    second_map = softmax_maps[:, 1] * (-lam_cols * value_dot - term_cols[:, 1, :, None])
    dscore = (jnp.stack([first_map, second_map], axis=1) * factor).astype(jnp.bfloat16)
    return (weights, dscore)


def block_span():
    return block_rows


def per_device(
    queries, key_vectors, latents, w_value, log_sums, out_pair, cotangent, lambdas, out_gain
):
    tok_rows = queries.shape[0]
    head_count = lambdas.shape[0]
    offset = lax.axis_index("sp") * tok_rows
    own_pos = offset + jnp.arange(tok_rows, dtype=jnp.int32)
    last_pos = offset + tok_rows - 1
    gathered = lax.all_gather(latents, "tp", axis=1, tiled=True)
    values = jnp.dot(gathered, w_value, preferred_element_type=jnp.float32).astype(jnp.bfloat16)
    out_grad, row_terms = head_cotangent(out_pair, cotangent, lambdas, out_gain)
    query_heads = queries.reshape(tok_rows, head_count, 2, -1)
    key_heads = key_vectors.reshape(tok_rows, head_count, 2, -1)
    value_heads = values.reshape(tok_rows, head_count, -1)
    log_heads = log_sums.reshape(tok_rows, head_count, 2)
    grad_flat = out_grad.reshape(tok_rows, -1)
    term_flat = row_terms.reshape(tok_rows, -1)
    zero_keys = jnp.zeros(key_heads.shape, jnp.float32)
    zero_values = jnp.zeros(value_heads.shape, jnp.float32)
    shards = (
        lax.all_gather(key_vectors, "sp", axis=0, tiled=True),
        lax.all_gather(values, "sp", axis=0, tiled=True),
    )
    key_piece = shards[0]
    value_piece = shards[1]
    piece_rows = key_piece.shape[0]
    block_len = block_span()

    def query_add_block(block_idx, partial_value):
        begin_row = block_idx * block_len
        key_block = lax.dynamic_slice_in_dim(key_piece, begin_row, block_len, 0).reshape(
            block_len, head_count, 2, -1
        )
        value_block = lax.dynamic_slice_in_dim(value_piece, begin_row, block_len, 0).reshape(
            block_len, head_count, -1
        )
        key_pos = begin_row + jnp.arange(block_len, dtype=jnp.int32)

        def query_compute(sums):
            weights, dscore = block_terms(
                query_heads,
                key_block,
                value_block,
                out_grad,
                log_heads,
                row_terms,
                lambdas,
                own_pos,
                key_pos,
            )
            return sums + jnp.einsum(
                "hcqk,khcd->qhcd", dscore, key_block, preferred_element_type=jnp.float32
            )

        return lax.cond(begin_row <= last_pos, query_compute, lambda sums: sums, partial_value)

    query_grad = lax.fori_loop(0, piece_rows // block_len, query_add_block, zero_keys)
    shards = (
        lax.all_gather(queries.astype(jnp.float32), "sp", axis=0, tiled=True).astype(jnp.bfloat16),
        lax.all_gather(grad_flat.astype(jnp.float32), "sp", axis=0, tiled=True).astype(
            jnp.bfloat16
        ),
        lax.all_gather(log_sums, "sp", axis=0, tiled=True),
        lax.all_gather(term_flat, "sp", axis=0, tiled=True),
    )
    query_piece = shards[0]
    grad_piece = shards[1]
    log_piece = shards[2]
    term_piece = shards[3]
    piece_rows = query_piece.shape[0]
    key_block_len = block_span()

    def key_add_block(block_idx, partial_value):
        begin_row = block_idx * key_block_len
        query_block = lax.dynamic_slice_in_dim(query_piece, begin_row, key_block_len, 0).reshape(
            key_block_len, head_count, 2, -1
        )
        grad_block = lax.dynamic_slice_in_dim(grad_piece, begin_row, key_block_len, 0).reshape(
            key_block_len, head_count, -1
        )
        log_block = lax.dynamic_slice_in_dim(log_piece, begin_row, key_block_len, 0).reshape(
            key_block_len, head_count, 2
        )
        term_block = lax.dynamic_slice_in_dim(term_piece, begin_row, key_block_len, 0).reshape(
            key_block_len, head_count, 2
        )
        query_pos = begin_row + jnp.arange(key_block_len, dtype=jnp.int32)

        def key_compute(sums):
            weights, dscore = block_terms(
                query_block,
                key_heads,
                value_heads,
                grad_block,
                log_block,
                term_block,
                lambdas,
                query_pos,
                own_pos,
            )
            key_sum = sums[0] + jnp.einsum(
                "hcqk,qhcd->khcd", dscore, query_block, preferred_element_type=jnp.float32
            )
            value_sum = sums[1] + jnp.einsum(
                "hqk,qhe->khe", weights, grad_block, preferred_element_type=jnp.float32
            )
            return (key_sum, value_sum)

        return lax.cond(
            begin_row + key_block_len - 1 >= offset, key_compute, lambda sums: sums, partial_value
        )

    key_grad, value_grad = lax.fori_loop(
        0, piece_rows // key_block_len, key_add_block, (zero_keys, zero_values)
    )
    value_flat = value_grad.reshape(tok_rows, -1)
    value_narrow = value_flat.astype(jnp.bfloat16)
    weight_grad = lax.psum_scatter(
        lax.dot_general(
            gathered, value_narrow, (((0,), (0,)), ((), ())), preferred_element_type=jnp.float32
        ),
        "sp",
        scatter_dimension=0,
        tiled=True,
    )
    return (
        query_grad.reshape(tok_rows, -1),
        key_grad.reshape(tok_rows, -1),
        value_flat,
        weight_grad,
    )


def solution(mesh):
    return jax.shard_map(
        per_device,
        mesh=mesh,
        in_specs=(
            P("sp", "tp"),
            P("sp", "tp"),
            P("sp", "tp"),
            P(None, "tp"),
            P("sp", "tp"),
            P("sp", "tp"),
            P("sp", "tp"),
            P("tp"),
            P(),
        ),
        out_specs=(P("sp", "tp"), P("sp", "tp"), P("sp", "tp"), P("sp", "tp")),
        check_vma=False,
    )
```

profile of v0, /device:TPU:0, one launch (start us, length us, event | category | flops | bytes accessed | tf_op | source)
XLA Modules:
  0.0 320.5 jit_solution(6820730226512585887)
XLA Ops:
  14.8 20.2 %all-gather.8.cloned.1.call-done = bf16[512,2048]{1,0:T(8,128)(2,1)} async-done(((bf16[512,512]{1,0:T(8,128)(2,1)}), bf16[512,2048]{1,0:T(8,128)(2,1)}) %all-gather.8.cloned.1.call-update) | async-done | bytes 2097168 | tf_op jit(solution)/shard_map/all_gather | solution.py:71
  38.7 31.0 %all_gather.25 = f32[4096,4]{0,1:T(4,128)S(1)} all-gather(f32[512,4]{0,1:T(4,128)S(1)} %copy-done.6), channel_id=1, replica_groups=mesh['sp'=8,'tp'=4] {'sp'}, dimensions={0}, use_global_device_ids=true | all-gather | bytes 73728 | tf_op jit(solution)/shard_map/all_gather | solution.py:125
  69.7 31.9 %all_gather.27 = f32[4096,4]{0,1:T(4,128)} all-gather(f32[512,4]{0,1:T(4,128)S(1)} %reshape.188), channel_id=1, replica_groups=mesh['sp'=8,'tp'=4] {'sp'}, dimensions={0}, use_global_device_ids=true | all-gather | bytes 73728 | tf_op jit(solution)/shard_map/all_gather | solution.py:126
  102.8 37.0 %all-gather.14.cloned.1.call-done = bf16[4096,256]{0,1:T(8,128)(2,1)} async-done(((bf16[512,256]{0,1:T(8,128)(2,1)}), bf16[4096,256]{0,1:T(8,128)(2,1)}) %all-gather.14.cloned.1.call-update) | async-done | bytes 2097168 | tf_op jit(solution)/shard_map/all_gather | solution.py:122
  139.9 90.7 %while.39 = (s32[]{:T(128)}, f32[512,2,2,64]{0,3,2,1:T(8,128)S(1)}, f32[512,2,128]{2,0,1:T(8,128)S(1)}, s32[]{:T(128)}, bf16[4096,256]{0,1:T(8,128)(2,1)}, /*ind...) while((s32[]{:T(128)}, f32[512,2,2,64]{0,3,2,1:T(8,128)S(1)}, ...), condition=%wide.region_11.12_spmd.clone.clone, body=%wide.region_8.11_spmd.clone.clone.sunk | while | flops 547881984 | bytes 43121072 | solution.py:175
  140.0 11.3 %conditional.8 = ((f32[512,2,2,64]{0,3,2,1:T(8,128)S(1)}, f32[512,2,128]{2,0,1:T(8,128)S(1)})) conditional(s32[]{:T(128)} %convert_element_type.110, (f32[512,2,2,64]{0,3,2,1:T(8,128)S(1)}, f32[512,2,128]{2,0,1:T(8,128)S(1)}) %tuple.152, (s32[]{:T(128)}, s32[]{:T(128)}, s32[512]{0:T(512)S(1)}, bf16[4096,256]{0,1:T(8,128)(2,1)}, ...), branch_computations={%region_9.9_spmd, %region_10.10_spmd} | conditional | flops 547881984 | bytes 43118728 | solution.py:171
  142.0 3.2 exponential_select_fusion
  151.3 11.3 %conditional.8 = ((f32[512,2,2,64]{0,3,2,1:T(8,128)S(1)}, f32[512,2,128]{2,0,1:T(8,128)S(1)})) conditional(s32[]{:T(128)} %convert_element_type.110, (f32[512,2,2,64]{0,3,2,1:T(8,128)S(1)}, f32[512,2,128]{2,0,1:T(8,128)S(1)}) %tuple.152, (s32[]{:T(128)}, s32[]{:T(128)}, s32[512]{0:T(512)S(1)}, bf16[4096,256]{0,1:T(8,128)(2,1)}, ...), branch_computations={%region_9.9_spmd, %region_10.10_spmd} | conditional | flops 547881984 | bytes 43118728 | solution.py:171
  162.6 11.4 %conditional.8 = ((f32[512,2,2,64]{0,3,2,1:T(8,128)S(1)}, f32[512,2,128]{2,0,1:T(8,128)S(1)})) conditional(s32[]{:T(128)} %convert_element_type.110, (f32[512,2,2,64]{0,3,2,1:T(8,128)S(1)}, f32[512,2,128]{2,0,1:T(8,128)S(1)}) %tuple.152, (s32[]{:T(128)}, s32[]{:T(128)}, s32[512]{0:T(512)S(1)}, bf16[4096,256]{0,1:T(8,128)(2,1)}, ...), branch_computations={%region_9.9_spmd, %region_10.10_spmd} | conditional | flops 547881984 | bytes 43118728 | solution.py:171
  164.7 3.2 exponential_select_fusion
  174.1 11.3 %conditional.8 = ((f32[512,2,2,64]{0,3,2,1:T(8,128)S(1)}, f32[512,2,128]{2,0,1:T(8,128)S(1)})) conditional(s32[]{:T(128)} %convert_element_type.110, (f32[512,2,2,64]{0,3,2,1:T(8,128)S(1)}, f32[512,2,128]{2,0,1:T(8,128)S(1)}) %tuple.152, (s32[]{:T(128)}, s32[]{:T(128)}, s32[512]{0:T(512)S(1)}, bf16[4096,256]{0,1:T(8,128)(2,1)}, ...), branch_computations={%region_9.9_spmd, %region_10.10_spmd} | conditional | flops 547881984 | bytes 43118728 | solution.py:171
  176.1 3.2 exponential_select_fusion
  185.4 11.2 %conditional.8 = ((f32[512,2,2,64]{0,3,2,1:T(8,128)S(1)}, f32[512,2,128]{2,0,1:T(8,128)S(1)})) conditional(s32[]{:T(128)} %convert_element_type.110, (f32[512,2,2,64]{0,3,2,1:T(8,128)S(1)}, f32[512,2,128]{2,0,1:T(8,128)S(1)}) %tuple.152, (s32[]{:T(128)}, s32[]{:T(128)}, s32[512]{0:T(512)S(1)}, bf16[4096,256]{0,1:T(8,128)(2,1)}, ...), branch_computations={%region_9.9_spmd, %region_10.10_spmd} | conditional | flops 547881984 | bytes 43118728 | solution.py:171
  187.4 3.2 exponential_select_fusion
  196.7 11.3 %conditional.8 = ((f32[512,2,2,64]{0,3,2,1:T(8,128)S(1)}, f32[512,2,128]{2,0,1:T(8,128)S(1)})) conditional(s32[]{:T(128)} %convert_element_type.110, (f32[512,2,2,64]{0,3,2,1:T(8,128)S(1)}, f32[512,2,128]{2,0,1:T(8,128)S(1)}) %tuple.152, (s32[]{:T(128)}, s32[]{:T(128)}, s32[512]{0:T(512)S(1)}, bf16[4096,256]{0,1:T(8,128)(2,1)}, ...), branch_computations={%region_9.9_spmd, %region_10.10_spmd} | conditional | flops 547881984 | bytes 43118728 | solution.py:171
  208.0 11.2 %conditional.8 = ((f32[512,2,2,64]{0,3,2,1:T(8,128)S(1)}, f32[512,2,128]{2,0,1:T(8,128)S(1)})) conditional(s32[]{:T(128)} %convert_element_type.110, (f32[512,2,2,64]{0,3,2,1:T(8,128)S(1)}, f32[512,2,128]{2,0,1:T(8,128)S(1)}) %tuple.152, (s32[]{:T(128)}, s32[]{:T(128)}, s32[512]{0:T(512)S(1)}, bf16[4096,256]{0,1:T(8,128)(2,1)}, ...), branch_computations={%region_9.9_spmd, %region_10.10_spmd} | conditional | flops 547881984 | bytes 43118728 | solution.py:171
  210.1 3.2 exponential_select_fusion
  219.3 11.3 %conditional.8 = ((f32[512,2,2,64]{0,3,2,1:T(8,128)S(1)}, f32[512,2,128]{2,0,1:T(8,128)S(1)})) conditional(s32[]{:T(128)} %convert_element_type.110, (f32[512,2,2,64]{0,3,2,1:T(8,128)S(1)}, f32[512,2,128]{2,0,1:T(8,128)S(1)}) %tuple.152, (s32[]{:T(128)}, s32[]{:T(128)}, s32[512]{0:T(512)S(1)}, bf16[4096,256]{0,1:T(8,128)(2,1)}, ...), branch_computations={%region_9.9_spmd, %region_10.10_spmd} | conditional | flops 547881984 | bytes 43118728 | solution.py:171
  221.4 3.2 exponential_select_fusion
  230.7 3.9 %convolution_bitcast_fusion.1 = f32[2048,256]{0,1:T(8,128)} fusion(bf16[512,2048]{1,0:T(8,128)(2,1)} %all-gather.8.cloned.1.call-done, f32[512,256]{1,0:T(8,128)S(1)} %copy_bitcast_fusion.2), kind=kOutput, calls=%fused_computation.46 | convolution fusion | flops 537001984 | bytes 4718592 | tf_op jit(solution)/shard_map/dot_general | solution.py:181
  235.8 5.5 %all-gather.10.cloned.1.call-done = bf16[4096,256]{0,1:T(8,128)(2,1)} async-done(((bf16[512,256]{0,1:T(8,128)(2,1)}), bf16[4096,256]{0,1:T(8,128)(2,1)}) %all-gather.10.cloned.1.call-update) | async-done | bytes 2097168 | tf_op jit(solution)/shard_map/all_gather | solution.py:84
  241.4 4.3 %while.38 = (s32[]{:T(128)}, f32[512,2,2,64]{0,3,2,1:T(8,128)S(1)}, s32[]{:T(128)}, bf16[4096,256]{0,1:T(8,128)(2,1)}, bf16[512,2,2,64]{0,3,2,1:T(8,128)(2,1)S(1...) while((s32[]{:T(128)}, f32[512,2,2,64]{0,3,2,1:T(8,128)S(1)}, ...), condition=%wide.region_7.8_spmd.clone, body=%wide.region_4.7_spmd.clone.sunk | while | flops 411960320 | bytes 20756812 | solution.py:119
  241.4 3.9 %conditional.7 = (f32[512,2,2,64]{0,3,2,1:T(8,128)S(1)}) conditional(s32[]{:T(128)} %convert_element_type.109, f32[512,2,2,64]{0,3,2,1:T(8,128)S(1)} %get-tuple-element.1245, (s32[]{:T(128)}, s32[512]{0:T(512)S(1)}, s32[]{:T(128)}, bf16[4096,256]{0,1:T(8,128)(2,1)}, bf16[512,2,2,64]{0,3,2,1:T(8,128)(2,1)S(1)}, /*index=5*/f32[512,2,2]{0,2,1:T(2,128)S(1)}, ...), branch_computations={%region_5.0_spmd, %region_6.6_spmd} | conditional | flops 411960320 | bytes 20754510 | solution.py:117
  246.7 65.2 %reduce-scatter.2.cloned.1.call-done = f32[256,256]{0,1:T(8,128)} async-done(((f32[2048,256]{0,1:T(8,128)}), f32[256,256]{0,1:T(8,128)}) %reduce-scatter.2.cloned.1.call-update) | async-done | bytes 262160 | tf_op jit(solution)/shard_map/reduce_scatter | solution.py:180
  (210 shorter events, 91.0 us)
Async XLA Ops:
  7.2 27.7 %copy-start = (bf16[2048,256]{1,0:T(8,128)(2,1)S(1)}, bf16[2048,256]{1,0:T(8,128)(2,1)}, u32[]{:S(2)}) copy-start(bf16[2048,256]{1,0:T(8,128)(2,1)} %param.20) | copy-start | bytes 3145732
  7.2 3.9 %copy-start.5 = (bf16[512,256]{1,0:T(8,128)(2,1)S(1)}, bf16[512,256]{1,0:T(8,128)(2,1)}, u32[]{:S(2)}) copy-start(bf16[512,256]{1,0:T(8,128)(2,1)} %param.23) | copy-start | bytes 786436
  7.2 4.1 %copy-start.8 = (f32[128]{0:T(128)S(1)}, f32[128]{0:T(128)}, u32[]{:S(2)}) copy-start(f32[128]{0:T(128)} %param.25) | copy-start | bytes 1540
  7.2 4.1 %copy-start.7 = (f32[2]{0:T(128)S(1)}, f32[2]{0:T(128)}, u32[]{:S(2)}) copy-start(f32[2]{0:T(128)} %param.24) | copy-start | bytes 28
  7.2 27.7 %all-gather.8.cloned.1.call-start = ((), (), s32[]{:S(2)}) async-start(), calls=%async_computation.2 | async-start | bytes 2621440 | tf_op jit(solution)/shard_map/all_gather | solution.py:71
  7.9 94.8 %all-gather.12.cloned.1.call-start = ((), (), s32[]{:S(2)}) async-start(), calls=%async_computation.4 | async-start | bytes 2359296 | tf_op jit(solution)/shard_map/all_gather | solution.py:121
  9.8 130.0 %all-gather.14.cloned.1.call-start = ((), (), s32[]{:S(2)}) async-start(), calls=%async_computation.5 | async-start | bytes 2359296 | tf_op jit(solution)/shard_map/all_gather | solution.py:122
  12.8 222.9 %all-gather.6.cloned.1.call-start = ((), (), s32[]{:S(2)}) async-start(), calls=%async_computation.1 | async-start | bytes 2359296 | tf_op jit(solution)/shard_map/all_gather | solution.py:83
  14.7 226.6 %all-gather.10.cloned.1.call-start = ((), (), s32[]{:S(2)}) async-start(), calls=%async_computation.3 | async-start | bytes 2359296 | tf_op jit(solution)/shard_map/all_gather | solution.py:84
  38.0 0.7 copy-start.6
  38.0 101.9 %copy-start.4 = (bf16[512,256]{0,1:T(8,128)(2,1)S(1)}, bf16[512,256]{0,1:T(8,128)(2,1)}, u32[]{:S(2)}) copy-start(bf16[512,256]{0,1:T(8,128)(2,1)} %copy.47) | copy-start | bytes 786436
  38.0 273.8 %reduce-scatter.2.cloned.1.call-start = ((), (), s32[]{:S(2)}) async-start(), calls=%async_computation.6 | async-start | bytes 2359296 | tf_op jit(solution)/shard_map/reduce_scatter | solution.py:180
  148.2 2.3 copy-start.1
  159.6 2.2 copy-start.1
  171.0 2.2 copy-start.1
  182.3 2.2 copy-start.1
  193.6 2.2 copy-start.1
  204.9 2.2 copy-start.1
  216.2 2.2 copy-start.1
  227.6 2.2 copy-start.1
  230.7 3.9 %copy-start.2 = (f32[512,256]{1,0:T(8,128)}, f32[512,256]{1,0:T(8,128)S(1)}, u32[]{:S(2)}) copy-start(f32[512,256]{1,0:T(8,128)S(1)} %copy_bitcast_fusion.2) | copy-start | bytes 1572868
  234.6 6.8 %copy-start.3 = (bf16[512,256]{0,1:T(8,128)(2,1)S(1)}, bf16[512,256]{0,1:T(8,128)(2,1)}, u32[]{:S(2)}) copy-start(bf16[512,256]{0,1:T(8,128)(2,1)} %copy.48) | copy-start | bytes 786436
Sparse Core Ops, SparseCore 0:
  9.6 25.2 all-gather.7
  37.5 50.9 all-gather.11
  91.1 48.6 all-gather.13
  142.3 48.5 all-gather.5
  192.7 48.5 all-gather.9
  244.7 67.0 reduce-scatter.1
where the time goes:
time: 322 us; the launch traced here: 320 us
  waiting for transfers between devices  129 us (40%)
  matrix products  69.3 us (22%)
  blocking collectives  62.9 us (20%)
  local copies, waits for them, and re-layouts  39.8 us (12%)
  between operations  14.3 us (4%)
  other arithmetic  3.63 us (1%)
    reduce_scatter x1, waiting for transfers between devices, per_device(): lax.psum_scatter(lax.dot_general(gathered, value_narrow, (((0,), (0,)), (...  65.2 us
    all_gather x1, waiting for transfers between devices, per_device(): lax.all_gather(grad_flat.astype(jnp.float32), 'sp', axis=0, tiled=True)  37 us
    all_gather x1, blocking collectives, per_device(): lax.all_gather(term_flat, 'sp', axis=0, tiled=True)  31.9 us
    all_gather x1, blocking collectives, per_device(): lax.all_gather(log_sums, 'sp', axis=0, tiled=True)  31 us
    dot_general x9, matrix products, block_terms(): jnp.einsum('qhcd,khcd->hcqk', query_block, key_block, preferred_element_t...  26.6 us
    dot_general x9, matrix products, block_terms(): jnp.einsum('qhe,khe->hqk', grad_block, value_block, preferred_element_typ...  24.4 us
    all_gather x1, waiting for transfers between devices, per_device(): gathered = lax.all_gather(latents, 'tp', axis=1, tiled=True)  20.2 us
    cond x32, local copies, waits for them, and re-layouts  13.3 us
  transfers between devices with their start and end apart: 6, of which 4 were waited for; matrix products, arithmetic and copies ran while one was open for 30% of the time, Pallas kernels for 0%

commit v1 on v0

--- a/solution.py
+++ b/solution.py
@@ -68,7 +68,12 @@
     offset = lax.axis_index("sp") * tok_rows
     own_pos = offset + jnp.arange(tok_rows, dtype=jnp.int32)
     last_pos = offset + tok_rows - 1
-    gathered = lax.all_gather(latents, "tp", axis=1, tiled=True)
+    ring = [latents]
+    for hop in range(3):
+        ring.append(lax.ppermute(ring[-1], "tp", [(dev, (dev + 1) % 4) for dev in range(4)]))
+    gathered = jnp.roll(
+        jnp.concatenate(ring[::-1], axis=1), (lax.axis_index("tp") + 1) * ring[0].shape[1], axis=1
+    )
     values = jnp.dot(gathered, w_value, preferred_element_type=jnp.float32).astype(jnp.bfloat16)
     out_grad, row_terms = head_cotangent(out_pair, cotangent, lambdas, out_gain)
     query_heads = queries.reshape(tok_rows, head_count, 2, -1)

time: 322 us -> 295 us (0.916)
  waiting for transfers between devices: 129 us -> 100 us
    all_gather x1, waiting for transfers between devices: 37 us -> 0.02 us  [per_device(): lax.all_gather(grad_flat.astype(jnp.float32), 'sp', axis=0, tiled=True)]
    ppermute x0 -> x3, waiting for transfers between devices: none -> 26.4 us  [per_device(): lax.ppermute(ring[-1], 'tp', [(dev, (dev + 1) % 4) for dev in range(4)])]
    all_gather x1 -> x0, waiting for transfers between devices: 20.2 us -> none  [per_device(): gathered = lax.all_gather(latents, 'tp', axis=1, tiled=True)]
    unnamed x25 -> x43, local copies, waits for them, and re-layouts: 10.3 us -> 16.7 us
    dynamic_slice x8, local copies, waits for them, and re-layouts: 5.66 us -> 0.09 us  [key_add_block(): lax.dynamic_slice_in_dim(term_piece, begin_row, key_block_len, 0)]
    cond x32 -> x48, local copies, waits for them, and re-layouts: 13.3 us -> 13.3 us
  transfers between devices with their start and end apart: 6 -> 8, of which waited for: 4 -> 5; matrix products, arithmetic and copies ran while one was open for 30% -> 32% of each run, Pallas kernels for 0% -> 0%
where the time goes in v1:
time: 295 us; the launch traced here: 294 us
  waiting for transfers between devices  100 us (34%)
  matrix products  68.4 us (23%)
  blocking collectives  63.8 us (22%)
  local copies, waits for them, and re-layouts  40.6 us (14%)
  between operations  14.1 us (5%)
  other arithmetic  4.34 us (1%)
    reduce_scatter x1, waiting for transfers between devices, per_device(): lax.psum_scatter(lax.dot_general(gathered, value_narrow, (((0,), (0,)), (...  65.1 us
    all_gather x1, blocking collectives, per_device(): lax.all_gather(log_sums, 'sp', axis=0, tiled=True)  32.5 us
    all_gather x1, blocking collectives, per_device(): lax.all_gather(term_flat, 'sp', axis=0, tiled=True)  31.3 us
    dot_general x9, matrix products, block_terms(): jnp.einsum('qhcd,khcd->hcqk', query_block, key_block, preferred_element_t...  27.2 us
    ppermute x3, waiting for transfers between devices, per_device(): lax.ppermute(ring[-1], 'tp', [(dev, (dev + 1) % 4) for dev in range(4)])  26.4 us
    dot_general x9, matrix products, block_terms(): jnp.einsum('qhe,khe->hqk', grad_block, value_block, preferred_element_typ...  24.4 us
    unnamed x43, local copies, waits for them, and re-layouts  16.7 us
    cond x48, local copies, waits for them, and re-layouts  13.3 us
  transfers between devices with their start and end apart: 8, of which 5 were waited for; matrix products, arithmetic and copies ran while one was open for 32% of the time, Pallas kernels for 0%

profile of v1, /device:TPU:0, one launch (start us, length us, event | category | flops | bytes accessed | tf_op | source)
XLA Modules:
  0.0 293.8 jit_solution(17803534033266157389)
XLA Ops:
  15.6 8.8 %collective-permute-done = bf16[512,512]{1,0:T(8,128)(2,1)S(1)} collective-permute-done((bf16[512,512]{1,0:T(8,128)(2,1)S(1)}, bf16[512,512]{1,0:T(8,128)(2,1)S(1)}, u32[]{:S(2)}, u32[]{:S(2)}) %collective-permute-start) | collective-permute-done | bytes 524320 | tf_op jit(solution)/shard_map/ppermute | solution.py:73
  25.2 8.7 %collective-permute-done.1 = bf16[512,512]{1,0:T(8,128)(2,1)} collective-permute-done((bf16[512,512]{1,0:T(8,128)(2,1)S(1)}, bf16[512,512]{1,0:T(8,128)(2,1)}, u32[]{:S(2)}, u32[]{:S(2)}) %collective-permute-start.1) | collective-permute-done | bytes 524320 | tf_op jit(solution)/shard_map/ppermute | solution.py:73
  33.9 8.9 %collective-permute-done.2 = bf16[512,512]{1,0:T(8,128)(2,1)} collective-permute-done((bf16[512,512]{1,0:T(8,128)(2,1)}, bf16[512,512]{1,0:T(8,128)(2,1)}, u32[]{:S(2)}, u32[]{:S(2)}) %collective-permute-start.2) | collective-permute-done | bytes 524320 | tf_op jit(solution)/shard_map/ppermute | solution.py:73
  52.2 32.5 %all_gather.21 = f32[4096,4]{0,1:T(4,128)S(1)} all-gather(f32[512,4]{0,1:T(4,128)S(1)} %copy-done.11), channel_id=1, replica_groups=mesh['sp'=8,'tp'=4] {'sp'}, dimensions={0}, use_global_device_ids=true | all-gather | bytes 73728 | tf_op jit(solution)/shard_map/all_gather | solution.py:130
  84.7 31.3 %all_gather.23 = f32[4096,4]{0,1:T(4,128)S(1)} all-gather(f32[512,4]{0,1:T(4,128)S(1)} %reshape.188), channel_id=1, replica_groups=mesh['sp'=8,'tp'=4] {'sp'}, dimensions={0}, use_global_device_ids=true | all-gather | bytes 73728 | tf_op jit(solution)/shard_map/all_gather | solution.py:131
  116.4 85.9 %while.39 = (s32[]{:T(128)}, f32[512,2,2,64]{0,3,2,1:T(8,128)S(1)}, f32[512,2,128]{2,0,1:T(8,128)S(1)}, s32[]{:T(128)}, bf16[4096,256]{0,1:T(8,128)(2,1)}, /*ind...) while((s32[]{:T(128)}, f32[512,2,2,64]{0,3,2,1:T(8,128)S(1)}, ...), condition=%wide.region_11.12_spmd.clone.clone, body=%wide.region_8.11_spmd.clone.clone.sunk | while | flops 547881984 | bytes 43121128 | solution.py:180
  116.4 10.8 %conditional.8 = ((f32[512,2,2,64]{0,3,2,1:T(8,128)S(1)}, f32[512,2,128]{2,0,1:T(8,128)S(1)})) conditional(s32[]{:T(128)} %convert_element_type.110, (f32[512,2,2,64]{0,3,2,1:T(8,128)S(1)}, f32[512,2,128]{2,0,1:T(8,128)S(1)}) %tuple.151, (s32[]{:T(128)}, s32[]{:T(128)}, s32[512]{0:T(512)S(1)}, bf16[4096,256]{0,1:T(8,128)(2,1)}, ...), branch_computations={%region_9.9_spmd, %region_10.10_spmd} | conditional | flops 547881984 | bytes 43118784 | solution.py:176
  127.2 10.7 %conditional.8 = ((f32[512,2,2,64]{0,3,2,1:T(8,128)S(1)}, f32[512,2,128]{2,0,1:T(8,128)S(1)})) conditional(s32[]{:T(128)} %convert_element_type.110, (f32[512,2,2,64]{0,3,2,1:T(8,128)S(1)}, f32[512,2,128]{2,0,1:T(8,128)S(1)}) %tuple.151, (s32[]{:T(128)}, s32[]{:T(128)}, s32[512]{0:T(512)S(1)}, bf16[4096,256]{0,1:T(8,128)(2,1)}, ...), branch_computations={%region_9.9_spmd, %region_10.10_spmd} | conditional | flops 547881984 | bytes 43118784 | solution.py:176
  137.9 10.8 %conditional.8 = ((f32[512,2,2,64]{0,3,2,1:T(8,128)S(1)}, f32[512,2,128]{2,0,1:T(8,128)S(1)})) conditional(s32[]{:T(128)} %convert_element_type.110, (f32[512,2,2,64]{0,3,2,1:T(8,128)S(1)}, f32[512,2,128]{2,0,1:T(8,128)S(1)}) %tuple.151, (s32[]{:T(128)}, s32[]{:T(128)}, s32[512]{0:T(512)S(1)}, bf16[4096,256]{0,1:T(8,128)(2,1)}, ...), branch_computations={%region_9.9_spmd, %region_10.10_spmd} | conditional | flops 547881984 | bytes 43118784 | solution.py:176
  139.3 3.2 %exponential_select_fusion = f32[2,2,512,512]{3,2,1,0:T(8,128)} fusion(bf16[512,2,2,64]{0,3,2,1:T(8,128)(2,1)S(1)} %bitcast.167, bf16[512,2,2,64]{0,3,2,1:T(8,128)(2,1)S(1)} %get-tuple-element.842, f32[2,2,512]{2,1,0:T(2,128)S(1)} %bitcast.180, pred[512,512]{1,0:T(8,128)(4,1)S(1)} %broadcast_compare_fusion.1), kind=kOutput, calls=%fused_computation.24 | convolution fusion | flops 137363456 | bytes 4988928 | tf_op jit(solution)/shard_map/while/body/eval_jaxpr/cond/branch_1_fun/qhcd,khcd->hcqk/dot_general | solution.py:41
  148.8 10.7 %conditional.8 = ((f32[512,2,2,64]{0,3,2,1:T(8,128)S(1)}, f32[512,2,128]{2,0,1:T(8,128)S(1)})) conditional(s32[]{:T(128)} %convert_element_type.110, (f32[512,2,2,64]{0,3,2,1:T(8,128)S(1)}, f32[512,2,128]{2,0,1:T(8,128)S(1)}) %tuple.151, (s32[]{:T(128)}, s32[]{:T(128)}, s32[512]{0:T(512)S(1)}, bf16[4096,256]{0,1:T(8,128)(2,1)}, ...), branch_computations={%region_9.9_spmd, %region_10.10_spmd} | conditional | flops 547881984 | bytes 43118784 | solution.py:176
  150.2 3.2 %exponential_select_fusion = f32[2,2,512,512]{3,2,1,0:T(8,128)} fusion(bf16[512,2,2,64]{0,3,2,1:T(8,128)(2,1)S(1)} %bitcast.167, bf16[512,2,2,64]{0,3,2,1:T(8,128)(2,1)S(1)} %get-tuple-element.842, f32[2,2,512]{2,1,0:T(2,128)S(1)} %bitcast.180, pred[512,512]{1,0:T(8,128)(4,1)S(1)} %broadcast_compare_fusion.1), kind=kOutput, calls=%fused_computation.24 | convolution fusion | flops 137363456 | bytes 4988928 | tf_op jit(solution)/shard_map/while/body/eval_jaxpr/cond/branch_1_fun/qhcd,khcd->hcqk/dot_general | solution.py:41
  159.5 10.7 %conditional.8 = ((f32[512,2,2,64]{0,3,2,1:T(8,128)S(1)}, f32[512,2,128]{2,0,1:T(8,128)S(1)})) conditional(s32[]{:T(128)} %convert_element_type.110, (f32[512,2,2,64]{0,3,2,1:T(8,128)S(1)}, f32[512,2,128]{2,0,1:T(8,128)S(1)}) %tuple.151, (s32[]{:T(128)}, s32[]{:T(128)}, s32[512]{0:T(512)S(1)}, bf16[4096,256]{0,1:T(8,128)(2,1)}, ...), branch_computations={%region_9.9_spmd, %region_10.10_spmd} | conditional | flops 547881984 | bytes 43118784 | solution.py:176
  160.9 3.2 %exponential_select_fusion = f32[2,2,512,512]{3,2,1,0:T(8,128)} fusion(bf16[512,2,2,64]{0,3,2,1:T(8,128)(2,1)S(1)} %bitcast.167, bf16[512,2,2,64]{0,3,2,1:T(8,128)(2,1)S(1)} %get-tuple-element.842, f32[2,2,512]{2,1,0:T(2,128)S(1)} %bitcast.180, pred[512,512]{1,0:T(8,128)(4,1)S(1)} %broadcast_compare_fusion.1), kind=kOutput, calls=%fused_computation.24 | convolution fusion | flops 137363456 | bytes 4988928 | tf_op jit(solution)/shard_map/while/body/eval_jaxpr/cond/branch_1_fun/qhcd,khcd->hcqk/dot_general | solution.py:41
  170.2 10.7 %conditional.8 = ((f32[512,2,2,64]{0,3,2,1:T(8,128)S(1)}, f32[512,2,128]{2,0,1:T(8,128)S(1)})) conditional(s32[]{:T(128)} %convert_element_type.110, (f32[512,2,2,64]{0,3,2,1:T(8,128)S(1)}, f32[512,2,128]{2,0,1:T(8,128)S(1)}) %tuple.151, (s32[]{:T(128)}, s32[]{:T(128)}, s32[512]{0:T(512)S(1)}, bf16[4096,256]{0,1:T(8,128)(2,1)}, ...), branch_computations={%region_9.9_spmd, %region_10.10_spmd} | conditional | flops 547881984 | bytes 43118784 | solution.py:176
  171.6 3.2 %exponential_select_fusion = f32[2,2,512,512]{3,2,1,0:T(8,128)} fusion(bf16[512,2,2,64]{0,3,2,1:T(8,128)(2,1)S(1)} %bitcast.167, bf16[512,2,2,64]{0,3,2,1:T(8,128)(2,1)S(1)} %get-tuple-element.842, f32[2,2,512]{2,1,0:T(2,128)S(1)} %bitcast.180, pred[512,512]{1,0:T(8,128)(4,1)S(1)} %broadcast_compare_fusion.1), kind=kOutput, calls=%fused_computation.24 | convolution fusion | flops 137363456 | bytes 4988928 | tf_op jit(solution)/shard_map/while/body/eval_jaxpr/cond/branch_1_fun/qhcd,khcd->hcqk/dot_general | solution.py:41
  180.9 10.7 %conditional.8 = ((f32[512,2,2,64]{0,3,2,1:T(8,128)S(1)}, f32[512,2,128]{2,0,1:T(8,128)S(1)})) conditional(s32[]{:T(128)} %convert_element_type.110, (f32[512,2,2,64]{0,3,2,1:T(8,128)S(1)}, f32[512,2,128]{2,0,1:T(8,128)S(1)}) %tuple.151, (s32[]{:T(128)}, s32[]{:T(128)}, s32[512]{0:T(512)S(1)}, bf16[4096,256]{0,1:T(8,128)(2,1)}, ...), branch_computations={%region_9.9_spmd, %region_10.10_spmd} | conditional | flops 547881984 | bytes 43118784 | solution.py:176
  182.3 3.2 %exponential_select_fusion = f32[2,2,512,512]{3,2,1,0:T(8,128)} fusion(bf16[512,2,2,64]{0,3,2,1:T(8,128)(2,1)S(1)} %bitcast.167, bf16[512,2,2,64]{0,3,2,1:T(8,128)(2,1)S(1)} %get-tuple-element.842, f32[2,2,512]{2,1,0:T(2,128)S(1)} %bitcast.180, pred[512,512]{1,0:T(8,128)(4,1)S(1)} %broadcast_compare_fusion.1), kind=kOutput, calls=%fused_computation.24 | convolution fusion | flops 137363456 | bytes 4988928 | tf_op jit(solution)/shard_map/while/body/eval_jaxpr/cond/branch_1_fun/qhcd,khcd->hcqk/dot_general | solution.py:41
  191.7 10.7 %conditional.8 = ((f32[512,2,2,64]{0,3,2,1:T(8,128)S(1)}, f32[512,2,128]{2,0,1:T(8,128)S(1)})) conditional(s32[]{:T(128)} %convert_element_type.110, (f32[512,2,2,64]{0,3,2,1:T(8,128)S(1)}, f32[512,2,128]{2,0,1:T(8,128)S(1)}) %tuple.151, (s32[]{:T(128)}, s32[]{:T(128)}, s32[512]{0:T(512)S(1)}, bf16[4096,256]{0,1:T(8,128)(2,1)}, ...), branch_computations={%region_9.9_spmd, %region_10.10_spmd} | conditional | flops 547881984 | bytes 43118784 | solution.py:176
  202.4 3.9 %fusion.28 = f32[2048,256]{1,0:T(8,128)} fusion(bf16[512,4096]{1,0:T(8,128)(2,1)} %copy-done.10, s32[]{:T(128)S(6)} %select_n.52, f32[512,256]{1,0:T(8,128)S(1)} %copy_bitcast_fusion.2), kind=kOutput, calls=%fused_computation.46 | convolution fusion | flops 537001984 | bytes 4718596 | tf_op jit(solution)/shard_map/dot_general | solution.py:186
  208.4 8.3 %all-gather.7.cloned.1.call-done = bf16[4096,256]{0,1:T(8,128)(2,1)} async-done(((bf16[512,256]{0,1:T(8,128)(2,1)}), bf16[4096,256]{0,1:T(8,128)(2,1)}) %all-gather.7.cloned.1.call-update) | async-done | bytes 2097168 | tf_op jit(solution)/shard_map/all_gather | solution.py:89
  216.9 4.3 %while.38 = (s32[]{:T(128)}, f32[512,2,2,64]{0,3,2,1:T(8,128)S(1)}, s32[]{:T(128)}, bf16[4096,256]{0,1:T(8,128)(2,1)}, bf16[512,2,2,64]{0,3,2,1:T(8,128)(2,1)S(1...) while((s32[]{:T(128)}, f32[512,2,2,64]{0,3,2,1:T(8,128)S(1)}, ...), condition=%wide.region_7.8_spmd.clone, body=%wide.region_4.7_spmd.clone.sunk | while | flops 411960320 | bytes 20756812 | solution.py:124
  216.9 3.9 %conditional.7 = (f32[512,2,2,64]{0,3,2,1:T(8,128)S(1)}) conditional(s32[]{:T(128)} %convert_element_type.109, f32[512,2,2,64]{0,3,2,1:T(8,128)S(1)} %get-tuple-element.1241, (s32[]{:T(128)}, s32[512]{0:T(512)S(1)}, s32[]{:T(128)}, bf16[4096,256]{0,1:T(8,128)(2,1)}, bf16[512,2,2,64]{0,3,2,1:T(8,128)(2,1)S(1)}, /*index=5*/f32[512,2,2]{0,2,1:T(2,128)S(1)}, ...), branch_computations={%region_5.5_spmd, %region_6.6_spmd} | conditional | flops 411960320 | bytes 20754510 | solution.py:122
  222.2 65.1 %reduce-scatter.2.cloned.1.call-done = f32[256,256]{1,0:T(8,128)} async-done(((f32[2048,256]{1,0:T(8,128)}), f32[256,256]{1,0:T(8,128)}) %reduce-scatter.2.cloned.1.call-update) | async-done | bytes 262160 | tf_op jit(solution)/shard_map/reduce_scatter | solution.py:185
  (248 shorter events, 94.1 us)
Async XLA Ops:
  7.2 42.4 %copy-start = (bf16[2048,256]{1,0:T(8,128)(2,1)S(1)}, bf16[2048,256]{1,0:T(8,128)(2,1)}, u32[]{:S(2)}) copy-start(bf16[2048,256]{1,0:T(8,128)(2,1)} %param.20) | copy-start | bytes 3145732
  7.2 4.4 %copy-start.15 = (f32[128]{0:T(128)S(1)}, f32[128]{0:T(128)}, u32[]{:S(2)}) copy-start(f32[128]{0:T(128)} %param.25) | copy-start | bytes 1540
  7.2 4.4 %copy-start.12 = (f32[2]{0:T(128)S(1)}, f32[2]{0:T(128)}, u32[]{:S(2)}) copy-start(f32[2]{0:T(128)} %param.24) | copy-start | bytes 28
  7.2 109.0 %all-gather.9.cloned.1.call-start = ((), (), s32[]{:S(2)}) async-start(), calls=%async_computation.3 | async-start | bytes 2359296 | tf_op jit(solution)/shard_map/all_gather | solution.py:126
  9.1 107.1 %all-gather.11.cloned.1.call-start = ((), (), s32[]{:S(2)}) async-start(), calls=%async_computation.4 | async-start | bytes 2359296 | tf_op jit(solution)/shard_map/all_gather | solution.py:127
  13.1 195.3 %all-gather.5.cloned.1.call-start = ((), (), s32[]{:S(2)}) async-start(), calls=%async_computation.1 | async-start | bytes 2359296 | tf_op jit(solution)/shard_map/all_gather | solution.py:88
  15.0 201.8 %all-gather.7.cloned.1.call-start = ((), (), s32[]{:S(2)}) async-start(), calls=%async_computation.2 | async-start | bytes 2359296 | tf_op jit(solution)/shard_map/all_gather | solution.py:89
  15.0 9.4 %collective-permute-start = (bf16[512,512]{1,0:T(8,128)(2,1)S(1)}, bf16[512,512]{1,0:T(8,128)(2,1)S(1)}, u32[]{:S(2)}, u32[]{:S(2)}) collective-permute-start(bf16[512,512]{1,0:T(8,128)(2,1)S(1)} %copy-done.2), channel_id=1, source_target_pairs={{0,1},{1,2},{2,3},{3,0},{4,5},{5,6},{6,7},{7,4},{8,9},{9,10},{10,1... | collective-permute-start | bytes 1572872 | tf_op jit(solution)/shard_map/ppermute | solution.py:73
  25.2 8.7 %collective-permute-start.1 = (bf16[512,512]{1,0:T(8,128)(2,1)S(1)}, bf16[512,512]{1,0:T(8,128)(2,1)}, u32[]{:S(2)}, u32[]{:S(2)}) collective-permute-start(bf16[512,512]{1,0:T(8,128)(2,1)S(1)} %collective-permute-done), channel_id=1, source_target_pairs={{0,1},{1,2},{2,3},{3,0},{4,5},{5,6},{6,7},{7,4},{8,9},{9,10},{10,1... | collective-permute-start | bytes 1572872 | tf_op jit(solution)/shard_map/ppermute | solution.py:73
  33.9 8.9 %collective-permute-start.2 = (bf16[512,512]{1,0:T(8,128)(2,1)}, bf16[512,512]{1,0:T(8,128)(2,1)}, u32[]{:S(2)}, u32[]{:S(2)}) collective-permute-start(bf16[512,512]{1,0:T(8,128)(2,1)} %collective-permute-done.1), channel_id=1, source_target_pairs={{0,1},{1,2},{2,3},{3,0},{4,5},{5,6},{6,7},{7,4},{8,9},{9,10},{10,1... | collective-permute-start | bytes 1572872 | tf_op jit(solution)/shard_map/ppermute | solution.py:73
  33.9 11.2 %copy-start.4 = (bf16[512,512]{1,0:T(8,128)(2,1)S(1)}, bf16[512,512]{1,0:T(8,128)(2,1)}, u32[]{:S(2)}) copy-start(bf16[512,512]{1,0:T(8,128)(2,1)} %copy-done.3) | copy-start | bytes 1572868
  51.0 65.0 %copy-start.8 = (bf16[512,256]{0,1:T(8,128)(2,1)S(1)}, bf16[512,256]{0,1:T(8,128)(2,1)}, u32[]{:S(2)}) copy-start(bf16[512,256]{0,1:T(8,128)(2,1)} %fusion.32) | copy-start | bytes 786436
  51.0 65.3 %copy-start.7 = (bf16[512,256]{0,1:T(8,128)(2,1)S(1)}, bf16[512,256]{0,1:T(8,128)(2,1)}, u32[]{:S(2)}) copy-start(bf16[512,256]{0,1:T(8,128)(2,1)} %copy.46) | copy-start | bytes 786436
  51.1 236.2 %reduce-scatter.2.cloned.1.call-start = ((), (), s32[]{:S(2)}) async-start(), calls=%async_computation.5 | async-start | bytes 2359296 | tf_op jit(solution)/shard_map/reduce_scatter | solution.py:185
  117.8 3.3 %copy-start.13 = (f32[2]{0:T(128)S(1)}, f32[2]{0:T(128)}, u32[]{:S(2)}) copy-start(f32[2]{0:T(128)} %get-tuple-element.847) | copy-start | bytes 28 | tf_op jit(solution)/shard_map/while/body/eval_jaxpr/cond
  139.3 3.3 %copy-start.13 = (f32[2]{0:T(128)S(1)}, f32[2]{0:T(128)}, u32[]{:S(2)}) copy-start(f32[2]{0:T(128)} %get-tuple-element.847) | copy-start | bytes 28 | tf_op jit(solution)/shard_map/while/body/eval_jaxpr/cond
  150.2 3.3 %copy-start.13 = (f32[2]{0:T(128)S(1)}, f32[2]{0:T(128)}, u32[]{:S(2)}) copy-start(f32[2]{0:T(128)} %get-tuple-element.847) | copy-start | bytes 28 | tf_op jit(solution)/shard_map/while/body/eval_jaxpr/cond
  160.9 3.3 %copy-start.13 = (f32[2]{0:T(128)S(1)}, f32[2]{0:T(128)}, u32[]{:S(2)}) copy-start(f32[2]{0:T(128)} %get-tuple-element.847) | copy-start | bytes 28 | tf_op jit(solution)/shard_map/while/body/eval_jaxpr/cond
  171.6 3.3 %copy-start.13 = (f32[2]{0:T(128)S(1)}, f32[2]{0:T(128)}, u32[]{:S(2)}) copy-start(f32[2]{0:T(128)} %get-tuple-element.847) | copy-start | bytes 28 | tf_op jit(solution)/shard_map/while/body/eval_jaxpr/cond
  182.3 3.3 %copy-start.13 = (f32[2]{0:T(128)S(1)}, f32[2]{0:T(128)}, u32[]{:S(2)}) copy-start(f32[2]{0:T(128)} %get-tuple-element.847) | copy-start | bytes 28 | tf_op jit(solution)/shard_map/while/body/eval_jaxpr/cond
  193.0 3.3 %copy-start.13 = (f32[2]{0:T(128)S(1)}, f32[2]{0:T(128)}, u32[]{:S(2)}) copy-start(f32[2]{0:T(128)} %get-tuple-element.847) | copy-start | bytes 28 | tf_op jit(solution)/shard_map/while/body/eval_jaxpr/cond
  202.4 3.9 %copy-start.9 = (f32[512,256]{1,0:T(8,128)}, f32[512,256]{1,0:T(8,128)S(1)}, u32[]{:S(2)}) copy-start(f32[512,256]{1,0:T(8,128)S(1)} %copy_bitcast_fusion.2) | copy-start | bytes 1572868
  206.3 10.5 %copy-start.6 = (bf16[512,256]{0,1:T(8,128)(2,1)S(1)}, bf16[512,256]{0,1:T(8,128)(2,1)}, u32[]{:S(2)}) copy-start(bf16[512,256]{0,1:T(8,128)(2,1)} %copy.47) | copy-start | bytes 786436
  206.3 10.5 %copy-start.14 = (f32[2]{0:T(128)S(1)}, f32[2]{0:T(128)}, u32[]{:S(2)}) copy-start(f32[2]{0:T(128)} %get-tuple-element.1334) | copy-start | bytes 28
  (14 other events, 28.7 us)
Sparse Core Ops, SparseCore 0:
  10.1 53.2 all-gather.8
  66.0 48.9 all-gather.10
  117.6 48.6 all-gather.4
  168.2 48.5 all-gather.6
  220.7 66.5 reduce-scatter.1
